TPU v7x, 32 devices: a whole 2x2x4 slice. The times are simulated.
32 devices in a mesh: rep: 2 (over x), fs: 8 (over z, y), tp: 2 (over core).
Axes of the slice: x: 2, y: 2, z: 4, core: 2. Of those that a mesh axis runs over, the one named last changes fastest.
Arguments:
- states: bfloat16 [6144, 2048], P(('rep', 'fs'), 'tp'), may hold values from -6 to 6
- mix_gain: float32 [2048], replicated, may hold values from 0.1 to 1.9
- w_value: bfloat16 [2048, 2048], P('fs', 'tp'), may hold values from -1 to 1
- w_gate: bfloat16 [2048, 2048], P('fs', 'tp'), may hold values from -0.125 to 0.125
- conv_kernel: float32 [31, 2048], replicated, may hold values from -1 to 1
- chan_gain: float32 [2048], replicated, may hold values from 0.1 to 1.9
- w_mix_out: bfloat16 [2048, 2048], P('fs', 'tp'), may hold values from -0.125 to 0.125
- mlp_gain: float32 [2048], replicated, may hold values from 0.1 to 1.9
- w_up: bfloat16 [2048, 6144], P('fs', 'tp'), may hold values from -0.125 to 0.125
- w_down_t: bfloat16 [2048, 6144], P('fs', 'tp'), may hold values from -0.078125 to 0.078125
Outputs:
- layer_out: bfloat16 [6144, 2048], P(('rep', 'fs'), 'tp')
All inputs are finite; a program needn't handle non-finite values.
Results may differ from a plain program's by a relative error of at most 0.017.
Values may be sent and summed in bfloat16 or wider, within the bound.
A program may use at most 64 MiB of HBM per device.

v0:
```python
import jax
import jax.numpy as jnp
from jax import lax
from jax.sharding import PartitionSpec as P

D = 2048
KWIDTH = 31
LENGTH = 128
EPS = 1e-06


def rms_norm(rows, gain):
    values = rows.astype(jnp.float32)
    scaled = values * lax.rsqrt(jnp.mean(values * values, axis=-1, keepdims=True) + EPS)
    return (scaled * gain).astype(jnp.bfloat16)


def times_transposed(left, right):
    return lax.dot_general(
        left, right, (((1,), (1,)), ((), ())), preferred_element_type=jnp.float32
    )


def body(
    states, mix_gain, w_value, w_gate, conv_kernel, chan_gain, w_mix_out, mlp_gain, w_up, w_down_t
):
    width = states.shape[1]
    offset = lax.axis_index("tp") * width
    token_rows = states.shape[0]
    whole_rows = lax.all_gather(states, "tp", axis=1, tiled=True)
    normed = rms_norm(whole_rows, mix_gain)
    columns = normed
    value = jnp.dot(
        columns,
        lax.all_gather(w_value, "fs", axis=0, tiled=True),
        preferred_element_type=jnp.float32,
    )
    gate = jnp.dot(
        columns,
        lax.all_gather(w_gate, "fs", axis=0, tiled=True),
        preferred_element_type=jnp.float32,
    )
    gated = value * jax.nn.sigmoid(gate)
    own_kernel = lax.dynamic_slice_in_dim(conv_kernel, offset, width, 1)
    blocks = gated.reshape(token_rows // LENGTH, LENGTH, width)
    padded = jnp.pad(blocks, ((0, 0), (KWIDTH - 1, 0), (0, 0)))
    filtered = jnp.zeros_like(blocks)
    for tap in range(KWIDTH):
        filtered = filtered + own_kernel[tap][None, None, :] * padded[:, tap : tap + LENGTH, :]
    filtered = filtered.reshape(token_rows, width)
    sum_rows, square_rows = lax.psum(
        (jnp.sum(filtered, axis=-1), jnp.sum(filtered * filtered, axis=-1)), "tp"
    )
    mean_rows = (sum_rows / D)[:, None]
    variance = (square_rows / D)[:, None] - mean_rows * mean_rows
    own_gain = lax.dynamic_slice_in_dim(chan_gain, offset, width, 0)
    activated = jax.nn.silu((filtered - mean_rows) * lax.rsqrt(variance + EPS) * own_gain).astype(
        jnp.bfloat16
    )
    mixer_terms = times_transposed(activated, lax.all_gather(w_mix_out, "fs", axis=0, tiled=True))
    mixed = lax.psum_scatter(
        mixer_terms.astype(jnp.bfloat16), "tp", scatter_dimension=1, tiled=True
    ).astype(jnp.float32)
    middle = (states.astype(jnp.float32) + mixed).astype(jnp.bfloat16)
    middle_rows = lax.all_gather(middle, "tp", axis=1, tiled=True)
    normed_mid = rms_norm(middle_rows, mlp_gain)
    columns = normed_mid
    upward = jnp.dot(
        columns, lax.all_gather(w_up, "fs", axis=0, tiled=True), preferred_element_type=jnp.float32
    )
    hidden = jnp.square(jnp.maximum(upward, 0.0)).astype(jnp.bfloat16)
    fed_terms = times_transposed(hidden, lax.all_gather(w_down_t, "fs", axis=0, tiled=True))
    fed = lax.psum_scatter(
        fed_terms.astype(jnp.bfloat16), "tp", scatter_dimension=1, tiled=True
    ).astype(jnp.float32)
    return (middle.astype(jnp.float32) + fed).astype(jnp.bfloat16)


def solution(mesh):
    in_specs = (
        P(("rep", "fs"), "tp"),
        P(),
        P("fs", "tp"),
        P("fs", "tp"),
        P(),
        P(),
        P("fs", "tp"),
        P(),
        P("fs", "tp"),
        P("fs", "tp"),
    )
    out_specs = P(("rep", "fs"), "tp")
    return jax.shard_map(body, mesh=mesh, in_specs=in_specs, out_specs=out_specs, check_vma=False)
```

profile of v0, /device:TPU:0, one launch (start us, length us, event | category | flops | bytes accessed | tf_op | source)
XLA Modules:
  0.0 658.4 jit_solution(12516439432388913050)
XLA Ops:
  6.5 0.7 all-gather.8.cloned.1.call-update
  7.3 0.7 all-gather.12.cloned.1.call-update
  8.1 0.7 all-gather.10.cloned.1.call-update
  8.8 0.5 all-gather.14.cloned.1.call-update
  9.3 0.0 reduce-scatter.3.cloned.1.call-start
  9.4 1.3 fusion.79
  10.7 1.5 constant_dynamic-slice_fusion
  12.2 9.2 %all-gather.8.cloned.1.call-done = bf16[384,2048]{1,0:T(8,128)(2,1)} async-done(((bf16[384,1024]{1,0:T(8,128)(2,1)}), bf16[384,2048]{1,0:T(8,128)(2,1)}) %all-gather.8.cloned.1.call-update) | async-done | bytes 1572880 | tf_op jit(solution)/shard_map/all_gather | solution.py:30
  21.4 1.9 fusion
  23.4 74.2 %all-gather.12.cloned.1.call-done = bf16[2048,1024]{1,0:T(8,128)(2,1)} async-done(((bf16[256,1024]{1,0:T(8,128)(2,1)}), bf16[2048,1024]{1,0:T(8,128)(2,1)}) %all-gather.12.cloned.1.call-update) | async-done | bytes 4194320 | tf_op jit(solution)/shard_map/all_gather | solution.py:40
  97.6 4.0 fusion.73
  101.6 69.5 %all-gather.10.cloned.1.call-done = bf16[2048,1024]{1,0:T(8,128)(2,1)} async-done(((bf16[256,1024]{1,0:T(8,128)(2,1)}), bf16[2048,1024]{1,0:T(8,128)(2,1)}) %all-gather.10.cloned.1.call-update) | async-done | bytes 4194320 | tf_op jit(solution)/shard_map/all_gather | solution.py:35
  171.0 4.1 divide_multiply_fusion
  175.2 7.0 %fusion.77 = (f32[3,128]{1,0:T(4,128)S(1)}, f32[3,128]{1,0:T(4,128)S(1)}, f32[3,128,1024]{2,1,0:T(8,128)S(1)}) fusion(f32[3,128,1024]{2,1,0:T(8,128)S(1)} %bitcast.48, f32[1024]{0:T(1024)S(1)} %bitcast.61, f32[1024]{0:T(1024)S(1)} %bitcast.63, f32[1024]{0:T(1024)S(1)} %bitcast.64, f32[1024]{0:T(1024)S(1)} %bitcast.65, f32[1024]{0:T(1024)S(1)} %bitcast.66, ...), kind=kLoop, calls=%fused_computation.120 | loop fusion | flops 25165056 | bytes 3275776 | tf_op jit(solution)/shard_map/reduce_sum | solution.py:52
  182.2 2.5 all-reduce.1
  184.7 0.6 multiply_convert_fusion.1
  185.2 59.1 %all-gather.14.cloned.1.call-done = bf16[2048,1024]{1,0:T(8,128)(2,1)} async-done(((bf16[256,1024]{1,0:T(8,128)(2,1)}), bf16[2048,1024]{1,0:T(8,128)(2,1)}) %all-gather.14.cloned.1.call-update) | async-done | bytes 4194320 | tf_op jit(solution)/shard_map/all_gather | solution.py:60
  244.4 5.2 convolution_convert_fusion
  249.6 0.0 all-gather.16.cloned.1.call-start
  249.7 7.6 %reduce-scatter.3.cloned.1.call-done = bf16[384,1024]{1,0:T(8,128)(2,1)} async-done(((bf16[384,2048]{1,0:T(8,128)(2,1)}), bf16[384,1024]{1,0:T(8,128)(2,1)}) %reduce-scatter.3.cloned.1.call-update) | async-done | bytes 786448 | tf_op jit(solution)/shard_map/reduce_scatter | solution.py:61
  257.3 2.3 add_convert_fusion.1
  259.6 0.0 all-gather.18.cloned.1.call-start
  259.6 0.7 all-gather.18.cloned.1.call-update
  260.4 0.7 all-gather.20.cloned.1.call-update
  261.1 0.2 reduce-scatter.5.cloned.1.call-start
  261.3 9.5 %all-gather.16.cloned.1.call-done = bf16[384,2048]{1,0:T(8,128)(2,1)} async-done(((bf16[384,1024]{1,0:T(8,128)(2,1)}), bf16[384,2048]{1,0:T(8,128)(2,1)}) %all-gather.16.cloned.1.call-update) | async-done | bytes 1572880 | tf_op jit(solution)/shard_map/all_gather | solution.py:65
  270.8 1.9 fusion.3
  272.8 177.6 %all-gather.18.cloned.1.call-done = bf16[2048,3072]{1,0:T(8,128)(2,1)} async-done(((bf16[256,3072]{1,0:T(8,128)(2,1)}), bf16[2048,3072]{1,0:T(8,128)(2,1)}) %all-gather.18.cloned.1.call-update) | async-done | bytes 12582928 | tf_op jit(solution)/shard_map/all_gather | solution.py:69
  450.3 176.5 %all-gather.20.cloned.1.call-done = bf16[2048,3072]{1,0:T(8,128)(2,1)} async-done(((bf16[256,3072]{1,0:T(8,128)(2,1)}), bf16[2048,3072]{1,0:T(8,128)(2,1)}) %all-gather.20.cloned.1.call-update) | async-done | bytes 12582928 | tf_op jit(solution)/shard_map/all_gather | solution.py:72
  626.8 15.3 %convolution_convert_fusion.1 = bf16[384,2048]{1,0:T(8,128)(2,1)} fusion(bf16[2048,3072]{1,0:T(8,128)(2,1)} %all-gather.20.cloned.1.call-done, bf16[2048,3072]{1,0:T(8,128)(2,1)} %all-gather.18.cloned.1.call-done, bf16[384,2048]{1,0:T(8,128)(2,1)S(1)} %copy-done.3, f32[2048]{0:T(1024)S(1)} %copy-done.5, f32[384]{0:T(512)S(1)} %add_rsqrt_fusion), kind=kOutput, calls=%fused_computation.42 | convolution fusion | flops 9671147520 | bytes 28321280 | tf_op jit(solution)/shard_map/dot_general | solution.py:19
  642.2 7.3 %reduce-scatter.5.cloned.1.call-done = bf16[384,1024]{1,0:T(8,128)(2,1)} async-done(((bf16[384,2048]{1,0:T(8,128)(2,1)}), bf16[384,1024]{1,0:T(8,128)(2,1)}) %reduce-scatter.5.cloned.1.call-update) | async-done | bytes 786448 | tf_op jit(solution)/shard_map/reduce_scatter | solution.py:73
  649.5 2.3 add_convert_fusion
  (25 shorter events, 0.3 us)
Async XLA Ops:
  6.5 14.9 %all-gather.8.cloned.1.call-start = ((), (), s32[]{:S(2)}) async-start(), calls=%async_computation.2 | async-start | bytes 2359296 | tf_op jit(solution)/shard_map/all_gather | solution.py:30
  7.3 90.3 %all-gather.12.cloned.1.call-start = ((), (), s32[]{:S(2)}) async-start(), calls=%async_computation.4 | async-start | bytes 4718592 | tf_op jit(solution)/shard_map/all_gather | solution.py:40
  8.0 89.6 %copy-start.4 = (f32[2048]{0:T(1024)S(1)}, f32[2048]{0:T(1024)}, u32[]{:S(2)}) copy-start(f32[2048]{0:T(1024)} %param.11) | copy-start | bytes 24580
  8.0 163.0 %all-gather.10.cloned.1.call-start = ((), (), s32[]{:S(2)}) async-start(), calls=%async_computation.3 | async-start | bytes 4718592 | tf_op jit(solution)/shard_map/all_gather | solution.py:35
  8.8 235.6 %all-gather.14.cloned.1.call-start = ((), (), s32[]{:S(2)}) async-start(), calls=%async_computation.5 | async-start | bytes 4718592 | tf_op jit(solution)/shard_map/all_gather | solution.py:60
  9.3 247.9 %reduce-scatter.3.cloned.1.call-start = ((), (), s32[]{:S(2)}) async-start(), calls=%async_computation.6 | async-start | bytes 2359296 | tf_op jit(solution)/shard_map/reduce_scatter | solution.py:61
  21.4 76.1 %copy-start.2 = (bf16[384,2048]{1,0:T(8,128)(2,1)S(1)}, bf16[384,2048]{1,0:T(8,128)(2,1)}, u32[]{:S(2)}) copy-start(bf16[384,2048]{1,0:T(8,128)(2,1)} %all-gather.8.cloned.1.call-done) | copy-start | bytes 4718596
  175.2 9.5 %dynamic-slice-start = ((f32[2048]{0:T(1024)}, s32[]{:T(128)}), f32[1024]{0:T(1024)S(1)}, s32[]{:S(2)}) async-start(f32[2048]{0:T(1024)} %param.15, s32[]{:T(128)} %select_n.4), calls=%async_computation.11 | async-start | bytes 8704 | tf_op jit(solution)/shard_map/dynamic_slice | solution.py:56
  249.6 7.7 %copy-start.1 = (bf16[384,1024]{1,0:T(8,128)(2,1)S(1)}, bf16[384,1024]{1,0:T(8,128)(2,1)}, u32[]{:S(2)}) copy-start(bf16[384,1024]{1,0:T(8,128)(2,1)} %param.10) | copy-start | bytes 2359300
  249.6 21.2 %all-gather.16.cloned.1.call-start = ((), (), s32[]{:S(2)}) async-start(), calls=%async_computation.7 | async-start | bytes 2359296 | tf_op jit(solution)/shard_map/all_gather | solution.py:65
  259.6 190.7 %all-gather.18.cloned.1.call-start = ((), (), s32[]{:S(2)}) async-start(), calls=%async_computation.8 | async-start | bytes 14155776 | tf_op jit(solution)/shard_map/all_gather | solution.py:69
  260.3 366.5 %copy-start.5 = (f32[2048]{0:T(1024)S(1)}, f32[2048]{0:T(1024)}, u32[]{:S(2)}) copy-start(f32[2048]{0:T(1024)} %param.17) | copy-start | bytes 24580
  260.4 366.5 %all-gather.20.cloned.1.call-start = ((), (), s32[]{:S(2)}) async-start(), calls=%async_computation.9 | async-start | bytes 14155776 | tf_op jit(solution)/shard_map/all_gather | solution.py:72
  261.1 388.4 %reduce-scatter.5.cloned.1.call-start = ((), (), s32[]{:S(2)}) async-start(), calls=%async_computation.10 | async-start | bytes 2359296 | tf_op jit(solution)/shard_map/reduce_scatter | solution.py:73
  270.8 356.0 %copy-start.3 = (bf16[384,2048]{1,0:T(8,128)(2,1)S(1)}, bf16[384,2048]{1,0:T(8,128)(2,1)}, u32[]{:S(2)}) copy-start(bf16[384,2048]{1,0:T(8,128)(2,1)} %all-gather.16.cloned.1.call-done) | copy-start | bytes 4718596
  642.2 7.3 %copy-start = (bf16[384,1024]{1,0:T(8,128)(2,1)S(1)}, bf16[384,1024]{1,0:T(8,128)(2,1)}, u32[]{:S(2)}) copy-start(bf16[384,1024]{1,0:T(8,128)(2,1)} %add_convert_fusion.1) | copy-start | bytes 2359300
Sparse Core Ops, SparseCore 0:
  8.9 12.5 all-gather.7
  23.6 73.9 all-gather.11
  99.7 71.3 all-gather.9
  173.0 71.3 all-gather.13
  249.7 7.4 reduce-scatter.2
  259.7 11.0 all-gather.15
  273.0 177.2 all-gather.17
  452.5 174.2 all-gather.19
  642.3 7.1 reduce-scatter.4
where the time goes:
time: 659 us; the launch traced here: 658 us
  waiting for transfers between devices  594 us (90%)
  matrix products  28.7 us (4%)
  other arithmetic  16.1 us (2%)
  between operations  13.3 us (2%)
    all_gather x1, waiting for transfers between devices, body(): lax.all_gather(w_up, 'fs', axis=0, tiled=True)  178 us
    all_gather x1, waiting for transfers between devices, body(): lax.all_gather(w_down_t, 'fs', axis=0, tiled=True)  176 us
    all_gather x1, waiting for transfers between devices, body(): lax.all_gather(w_gate, 'fs', axis=0, tiled=True)  74.2 us
    all_gather x1, waiting for transfers between devices, body(): lax.all_gather(w_value, 'fs', axis=0, tiled=True)  69.5 us
    all_gather x1, waiting for transfers between devices, body(): lax.all_gather(w_mix_out, 'fs', axis=0, tiled=True)  59.1 us
    dot_general x2, matrix products, times_transposed(): lax.dot_general(left, right, (((1,), (1,)), ((), ())), preferred_element_...  20.6 us
  transfers between devices with their start and end apart: 9, of which 9 were waited for; matrix products, arithmetic and copies ran while one was open for 3% of the time, Pallas kernels for 0%

commit v1 on v0

--- a/solution.py
+++ b/solution.py
@@ -7,6 +7,22 @@
 KWIDTH = 31
 LENGTH = 128
 EPS = 1e-06
+
+
+def gather_around(x, axis, dim):
+    ways, here, turn = (lax.axis_size(axis), lax.axis_index(axis), x.shape[dim])
+    shape = [n * ways if d == dim else n for d, n in enumerate(x.shape)]
+    full = lax.dynamic_update_slice_in_dim(jnp.zeros(shape, x.dtype), x, here * turn, axis=dim)
+    going_up = going_down = x
+    for far in range(1, ways // 2 + 1):
+        going_up = lax.ppermute(going_up, axis, [(d, (d + 1) % ways) for d in range(ways)])
+        full = lax.dynamic_update_slice_in_dim(full, going_up, (here - far) % ways * turn, axis=dim)
+        if 2 * far < ways:
+            going_down = lax.ppermute(going_down, axis, [(d, (d - 1) % ways) for d in range(ways)])
+            full = lax.dynamic_update_slice_in_dim(
+                full, going_down, (here + far) % ways * turn, axis=dim
+            )
+    return full
 
 
 def rms_norm(rows, gain):
@@ -30,11 +46,7 @@
     whole_rows = lax.all_gather(states, "tp", axis=1, tiled=True)
     normed = rms_norm(whole_rows, mix_gain)
     columns = normed
-    value = jnp.dot(
-        columns,
-        lax.all_gather(w_value, "fs", axis=0, tiled=True),
-        preferred_element_type=jnp.float32,
-    )
+    value = jnp.dot(columns, gather_around(w_value, "fs", 0), preferred_element_type=jnp.float32)
     gate = jnp.dot(
         columns,
         lax.all_gather(w_gate, "fs", axis=0, tiled=True),

time: 659 us -> 626 us (0.950)
  waiting for transfers between devices: 594 us -> 533 us
  starting transfers between devices: 0.49 us -> 19.4 us
  local copies, waits for them, and re-layouts: 2.87 us -> 12 us
    ppermute x0 -> x7, waiting for transfers between devices: none -> 77.8 us  [the longest x4 70.6 us: gather_around(): lax.ppermute(going_up, axis, [(d, (d + 1) % ways) for d in range(ways)])]
    all_gather x1 -> x0, waiting for transfers between devices: 69.5 us -> none  [body(): lax.all_gather(w_value, 'fs', axis=0, tiled=True)]
    all_gather x1, waiting for transfers between devices: 74.2 us -> 17.1 us  [body(): lax.all_gather(w_gate, 'fs', axis=0, tiled=True)]
    ppermute x0 -> x7, starting transfers between devices: none -> 19 us  [the longest x3 11 us: gather_around(): lax.ppermute(going_down, axis, [(d, (d - 1) % ways) for d in range(ways)])]
    all_gather x1, waiting for transfers between devices: 9.21 us -> 0.01 us  [body(): whole_rows = lax.all_gather(states, 'tp', axis=1, tiled=True)]
    dynamic_update_slice x0 -> x8, local copies, waits for them, and re-layouts: none -> 6.74 us  [the longest x4 3.33 us: gather_around(): lax.dynamic_update_slice_in_dim(full, going_up, (here - far) % ways * tur...]
  transfers between devices with their start and end apart: 9 -> 15, of which waited for: 9 -> 12; matrix products, arithmetic and copies ran while one was open for 3% -> 5% of each run, Pallas kernels for 0% -> 0%
where the time goes in v1:
time: 626 us
  waiting for transfers between devices  533 us (85%)
  matrix products  28.6 us (5%)
  starting transfers between devices  19.4 us (3%)
  other arithmetic  16.1 us (3%)
  between operations  13.7 us (2%)
  local copies, waits for them, and re-layouts  12 us (2%)
    all_gather x1, waiting for transfers between devices, body(): lax.all_gather(w_up, 'fs', axis=0, tiled=True)  177 us
    all_gather x1, waiting for transfers between devices, body(): lax.all_gather(w_down_t, 'fs', axis=0, tiled=True)  176 us
    ppermute x4, waiting for transfers between devices, gather_around(): lax.ppermute(going_up, axis, [(d, (d + 1) % ways) for d in range(ways)])  70.6 us
    all_gather x1, waiting for transfers between devices, body(): lax.all_gather(w_mix_out, 'fs', axis=0, tiled=True)  56.5 us
    dot_general x2, matrix products, times_transposed(): lax.dot_general(left, right, (((1,), (1,)), ((), ())), preferred_element_...  20.5 us
    all_gather x1, waiting for transfers between devices, body(): lax.all_gather(w_gate, 'fs', axis=0, tiled=True)  17.1 us
  transfers between devices with their start and end apart: 15, of which 12 were waited for; matrix products, arithmetic and copies ran while one was open for 5% of the time, Pallas kernels for 0%

profile of v1, /device:TPU:0, one launch (start us, length us, event | category | flops | bytes accessed | tf_op | source)
XLA Modules:
  0.0 625.6 jit_solution(15937728451691553155)
XLA Ops:
  8.8 3.0 collective-permute-start
  11.8 3.1 collective-permute-start.1
  15.0 21.1 %collective-permute-done = bf16[256,1024]{1,0:T(8,128)(2,1)S(1)} collective-permute-done((bf16[256,1024]{1,0:T(8,128)(2,1)S(1)}, bf16[256,1024]{1,0:T(8,128)(2,1)S(1)}, u32[]{:S(2)}, u32[]{:S(2)}) %collective-permute-start) | collective-permute-done | bytes 524320 | tf_op jit(solution)/shard_map/ppermute | solution.py:18
  36.1 2.5 collective-permute-start.2
  38.5 3.1 collective-permute-start.3
  41.6 1.5 constant_dynamic-slice_fusion
  43.1 2.5 broadcast_in_dim.2
  45.6 0.9 constant_dynamic-update-slice_fusion.7
  46.5 17.9 %collective-permute-done.2 = bf16[256,1024]{1,0:T(8,128)(2,1)S(1)} collective-permute-done((bf16[256,1024]{1,0:T(8,128)(2,1)S(1)}, bf16[256,1024]{1,0:T(8,128)(2,1)S(1)}, u32[]{:S(2)}, u32[]{:S(2)}) %collective-permute-start.2) | collective-permute-done | bytes 524320 | tf_op jit(solution)/shard_map/ppermute | solution.py:18
  64.4 1.3 fusion.79
  65.8 4.8 collective-permute-start.5
  73.9 24.0 %collective-permute-done.4 = bf16[256,1024]{1,0:T(8,128)(2,1)S(1)} collective-permute-done((bf16[256,1024]{1,0:T(8,128)(2,1)S(1)}, bf16[256,1024]{1,0:T(8,128)(2,1)S(1)}, u32[]{:S(2)}, u32[]{:S(2)}) %collective-permute-start.4) | collective-permute-done | bytes 524320 | tf_op jit(solution)/shard_map/ppermute | solution.py:18
  97.9 2.5 collective-permute-start.6
  101.3 7.2 %collective-permute-done.5 = bf16[256,1024]{1,0:T(8,128)(2,1)S(1)} collective-permute-done((bf16[256,1024]{1,0:T(8,128)(2,1)S(1)}, bf16[256,1024]{1,0:T(8,128)(2,1)S(1)}, u32[]{:S(2)}, u32[]{:S(2)}) %collective-permute-start.5) | collective-permute-done | bytes 524320 | tf_op jit(solution)/shard_map/ppermute | solution.py:21
  109.4 1.9 fusion
  111.3 7.6 %collective-permute-done.6 = bf16[256,1024]{1,0:T(8,128)(2,1)S(1)} collective-permute-done((bf16[256,1024]{1,0:T(8,128)(2,1)S(1)}, bf16[256,1024]{1,0:T(8,128)(2,1)S(1)}, u32[]{:S(2)}, u32[]{:S(2)}) %collective-permute-start.6) | collective-permute-done | bytes 524320 | tf_op jit(solution)/shard_map/ppermute | solution.py:18
  119.7 17.1 %all-gather.9.cloned.1.call-done = bf16[2048,1024]{1,0:T(8,128)(2,1)} async-done(((bf16[256,1024]{1,0:T(8,128)(2,1)}), bf16[2048,1024]{1,0:T(8,128)(2,1)}) %all-gather.9.cloned.1.call-update) | async-done | bytes 4194320 | tf_op jit(solution)/shard_map/all_gather | solution.py:52
  136.8 4.0 fusion.73
  140.9 4.1 divide_multiply_fusion
  145.0 7.0 %fusion.77 = (f32[3,128]{1,0:T(4,128)S(1)}, f32[3,128]{1,0:T(4,128)S(1)}, f32[3,128,1024]{2,1,0:T(8,128)S(1)}) fusion(f32[3,128,1024]{2,1,0:T(8,128)S(1)} %bitcast.48, f32[1024]{0:T(1024)S(1)} %bitcast.61, f32[1024]{0:T(1024)S(1)} %bitcast.63, f32[1024]{0:T(1024)S(1)} %bitcast.64, f32[1024]{0:T(1024)S(1)} %bitcast.65, f32[1024]{0:T(1024)S(1)} %bitcast.66, ...), kind=kLoop, calls=%fused_computation.128 | loop fusion | flops 25165056 | bytes 3275776 | tf_op jit(solution)/shard_map/reduce_sum | solution.py:64
  152.0 2.5 all-reduce.1
  155.1 56.5 %all-gather.11.cloned.1.call-done = bf16[2048,1024]{1,0:T(8,128)(2,1)} async-done(((bf16[256,1024]{1,0:T(8,128)(2,1)}), bf16[2048,1024]{1,0:T(8,128)(2,1)}) %all-gather.11.cloned.1.call-update) | async-done | bytes 4194320 | tf_op jit(solution)/shard_map/all_gather | solution.py:72
  211.5 5.2 convolution_convert_fusion
  216.8 7.6 %reduce-scatter.3.cloned.1.call-done = bf16[384,1024]{1,0:T(8,128)(2,1)} async-done(((bf16[384,2048]{1,0:T(8,128)(2,1)}), bf16[384,1024]{1,0:T(8,128)(2,1)}) %reduce-scatter.3.cloned.1.call-update) | async-done | bytes 786448 | tf_op jit(solution)/shard_map/reduce_scatter | solution.py:73
  224.4 2.3 add_convert_fusion.1
  228.3 9.7 %all-gather.13.cloned.1.call-done = bf16[384,2048]{1,0:T(8,128)(2,1)} async-done(((bf16[384,1024]{1,0:T(8,128)(2,1)}), bf16[384,2048]{1,0:T(8,128)(2,1)}) %all-gather.13.cloned.1.call-update) | async-done | bytes 1572880 | tf_op jit(solution)/shard_map/all_gather | solution.py:77
  237.9 1.9 fusion.3
  239.9 177.4 %all-gather.15.cloned.1.call-done = bf16[2048,3072]{1,0:T(8,128)(2,1)} async-done(((bf16[256,3072]{1,0:T(8,128)(2,1)}), bf16[2048,3072]{1,0:T(8,128)(2,1)}) %all-gather.15.cloned.1.call-update) | async-done | bytes 12582928 | tf_op jit(solution)/shard_map/all_gather | solution.py:81
  417.3 176.5 %all-gather.17.cloned.1.call-done = bf16[2048,3072]{1,0:T(8,128)(2,1)} async-done(((bf16[256,3072]{1,0:T(8,128)(2,1)}), bf16[2048,3072]{1,0:T(8,128)(2,1)}) %all-gather.17.cloned.1.call-update) | async-done | bytes 12582928 | tf_op jit(solution)/shard_map/all_gather | solution.py:84
  593.8 15.3 %convolution_convert_fusion.1 = bf16[384,2048]{1,0:T(8,128)(2,1)} fusion(bf16[2048,3072]{1,0:T(8,128)(2,1)} %all-gather.17.cloned.1.call-done, bf16[2048,3072]{1,0:T(8,128)(2,1)} %all-gather.15.cloned.1.call-done, bf16[384,2048]{1,0:T(8,128)(2,1)S(1)} %copy-done.3, f32[2048]{0:T(1024)S(1)} %copy-done.6, f32[384]{0:T(512)S(1)} %add_rsqrt_fusion), kind=kOutput, calls=%fused_computation.42 | convolution fusion | flops 9671147520 | bytes 28321280 | tf_op jit(solution)/shard_map/dot_general | solution.py:35
  609.2 7.3 %reduce-scatter.5.cloned.1.call-done = bf16[384,1024]{1,0:T(8,128)(2,1)} async-done(((bf16[384,2048]{1,0:T(8,128)(2,1)}), bf16[384,1024]{1,0:T(8,128)(2,1)}) %reduce-scatter.5.cloned.1.call-update) | async-done | bytes 786448 | tf_op jit(solution)/shard_map/reduce_scatter | solution.py:85
  616.4 2.3 add_convert_fusion
  (47 shorter events, 10.3 us)
Async XLA Ops:
  6.5 2.3 copy-start.4
  6.5 102.8 %all-gather.7.cloned.1.call-start = ((), (), s32[]{:S(2)}) async-start(), calls=%async_computation.2 | async-start | bytes 2359296 | tf_op jit(solution)/shard_map/all_gather | solution.py:46
  7.3 129.6 %all-gather.9.cloned.1.call-start = ((), (), s32[]{:S(2)}) async-start(), calls=%async_computation.3 | async-start | bytes 4718592 | tf_op jit(solution)/shard_map/all_gather | solution.py:52
  8.0 203.5 %all-gather.11.cloned.1.call-start = ((), (), s32[]{:S(2)}) async-start(), calls=%async_computation.4 | async-start | bytes 4718592 | tf_op jit(solution)/shard_map/all_gather | solution.py:72
  8.7 215.6 %reduce-scatter.3.cloned.1.call-start = ((), (), s32[]{:S(2)}) async-start(), calls=%async_computation.5 | async-start | bytes 2359296 | tf_op jit(solution)/shard_map/reduce_scatter | solution.py:73
  8.8 27.3 %collective-permute-start = (bf16[256,1024]{1,0:T(8,128)(2,1)S(1)}, bf16[256,1024]{1,0:T(8,128)(2,1)S(1)}, u32[]{:S(2)}, u32[]{:S(2)}) collective-permute-start(bf16[256,1024]{1,0:T(8,128)(2,1)S(1)} %copy-done.4), channel_id=1, source_target_pairs={{0,2},{2,4},{4,6},{6,8},{8,10},{10,12},{12,14},{14,0},{1,3},{3,5},... | collective-permute-start | bytes 1572872 | tf_op jit(solution)/shard_map/ppermute | solution.py:18
  11.8 26.7 %collective-permute-start.1 = (bf16[256,1024]{1,0:T(8,128)(2,1)S(1)}, bf16[256,1024]{1,0:T(8,128)(2,1)S(1)}, u32[]{:S(2)}, u32[]{:S(2)}) collective-permute-start(bf16[256,1024]{1,0:T(8,128)(2,1)S(1)} %copy-done.4), channel_id=1, source_target_pairs={{0,14},{2,0},{4,2},{6,4},{8,6},{10,8},{12,10},{14,12},{1,15},{3,1}... | collective-permute-start | bytes 1572872 | tf_op jit(solution)/shard_map/ppermute | solution.py:21
  36.1 28.3 %collective-permute-start.2 = (bf16[256,1024]{1,0:T(8,128)(2,1)S(1)}, bf16[256,1024]{1,0:T(8,128)(2,1)S(1)}, u32[]{:S(2)}, u32[]{:S(2)}) collective-permute-start(bf16[256,1024]{1,0:T(8,128)(2,1)S(1)} %collective-permute-done), channel_id=1, source_target_pairs={{0,2},{2,4},{4,6},{6,8},{8,10},{10,12},{12,14},{14,0},{1,3},{3,5},... | collective-permute-start | bytes 1572872 | tf_op jit(solution)/shard_map/ppermute | solution.py:18
  38.5 27.3 %collective-permute-start.3 = (bf16[256,1024]{1,0:T(8,128)(2,1)S(1)}, bf16[256,1024]{1,0:T(8,128)(2,1)S(1)}, u32[]{:S(2)}, u32[]{:S(2)}) collective-permute-start(bf16[256,1024]{1,0:T(8,128)(2,1)S(1)} %collective-permute-done.1), channel_id=1, source_target_pairs={{0,14},{2,0},{4,2},{6,4},{8,6},{10,8},{12,10},{14,12},{1,15},{3,1}... | collective-permute-start | bytes 1572872 | tf_op jit(solution)/shard_map/ppermute | solution.py:21
  64.4 33.5 %collective-permute-start.4 = (bf16[256,1024]{1,0:T(8,128)(2,1)S(1)}, bf16[256,1024]{1,0:T(8,128)(2,1)S(1)}, u32[]{:S(2)}, u32[]{:S(2)}) collective-permute-start(bf16[256,1024]{1,0:T(8,128)(2,1)S(1)} %collective-permute-done.2), channel_id=1, source_target_pairs={{0,2},{2,4},{4,6},{6,8},{8,10},{10,12},{12,14},{14,0},{1,3},{3,5},... | collective-permute-start | bytes 1572872 | tf_op jit(solution)/shard_map/ppermute | solution.py:18
  65.8 42.7 %collective-permute-start.5 = (bf16[256,1024]{1,0:T(8,128)(2,1)S(1)}, bf16[256,1024]{1,0:T(8,128)(2,1)S(1)}, u32[]{:S(2)}, u32[]{:S(2)}) collective-permute-start(bf16[256,1024]{1,0:T(8,128)(2,1)S(1)} %collective-permute-done.3), channel_id=1, source_target_pairs={{0,14},{2,0},{4,2},{6,4},{8,6},{10,8},{12,10},{14,12},{1,15},{3,1}... | collective-permute-start | bytes 1572872 | tf_op jit(solution)/shard_map/ppermute | solution.py:21
  97.9 20.9 %collective-permute-start.6 = (bf16[256,1024]{1,0:T(8,128)(2,1)S(1)}, bf16[256,1024]{1,0:T(8,128)(2,1)S(1)}, u32[]{:S(2)}, u32[]{:S(2)}) collective-permute-start(bf16[256,1024]{1,0:T(8,128)(2,1)S(1)} %collective-permute-done.4), channel_id=1, source_target_pairs={{0,2},{2,4},{4,6},{6,8},{8,10},{10,12},{12,14},{14,0},{1,3},{3,5},... | collective-permute-start | bytes 1572872 | tf_op jit(solution)/shard_map/ppermute | solution.py:18
  109.4 27.5 %copy-start.5 = (f32[2048]{0:T(1024)S(1)}, f32[2048]{0:T(1024)}, u32[]{:S(2)}) copy-start(f32[2048]{0:T(1024)} %param.11) | copy-start | bytes 24580
  109.4 27.5 %copy-start.2 = (bf16[384,2048]{1,0:T(8,128)(2,1)S(1)}, bf16[384,2048]{1,0:T(8,128)(2,1)}, u32[]{:S(2)}) copy-start(bf16[384,2048]{1,0:T(8,128)(2,1)} %all-gather.7.cloned.1.call-done) | copy-start | bytes 4718596
  145.0 9.5 %dynamic-slice-start = ((f32[2048]{0:T(1024)}, s32[]{:T(128)}), f32[1024]{0:T(1024)S(1)}, s32[]{:S(2)}) async-start(f32[2048]{0:T(1024)} %param.15, s32[]{:T(128)} %select_n.59), calls=%async_computation.10 | async-start | bytes 8704 | tf_op jit(solution)/shard_map/dynamic_slice | solution.py:68
  216.7 7.7 %copy-start.1 = (bf16[384,1024]{1,0:T(8,128)(2,1)S(1)}, bf16[384,1024]{1,0:T(8,128)(2,1)}, u32[]{:S(2)}) copy-start(bf16[384,1024]{1,0:T(8,128)(2,1)} %param.10) | copy-start | bytes 2359300
  216.7 21.2 %all-gather.13.cloned.1.call-start = ((), (), s32[]{:S(2)}) async-start(), calls=%async_computation.6 | async-start | bytes 2359296 | tf_op jit(solution)/shard_map/all_gather | solution.py:77
  226.7 190.6 %all-gather.15.cloned.1.call-start = ((), (), s32[]{:S(2)}) async-start(), calls=%async_computation.7 | async-start | bytes 14155776 | tf_op jit(solution)/shard_map/all_gather | solution.py:81
  227.3 366.5 %copy-start.6 = (f32[2048]{0:T(1024)S(1)}, f32[2048]{0:T(1024)}, u32[]{:S(2)}) copy-start(f32[2048]{0:T(1024)} %param.17) | copy-start | bytes 24580
  227.3 366.5 %all-gather.17.cloned.1.call-start = ((), (), s32[]{:S(2)}) async-start(), calls=%async_computation.8 | async-start | bytes 14155776 | tf_op jit(solution)/shard_map/all_gather | solution.py:84
  228.0 388.4 %reduce-scatter.5.cloned.1.call-start = ((), (), s32[]{:S(2)}) async-start(), calls=%async_computation.9 | async-start | bytes 2359296 | tf_op jit(solution)/shard_map/reduce_scatter | solution.py:85
  237.9 355.9 %copy-start.3 = (bf16[384,2048]{1,0:T(8,128)(2,1)S(1)}, bf16[384,2048]{1,0:T(8,128)(2,1)}, u32[]{:S(2)}) copy-start(bf16[384,2048]{1,0:T(8,128)(2,1)} %all-gather.13.cloned.1.call-done) | copy-start | bytes 4718596
  609.1 7.3 %copy-start = (bf16[384,1024]{1,0:T(8,128)(2,1)S(1)}, bf16[384,1024]{1,0:T(8,128)(2,1)}, u32[]{:S(2)}) copy-start(bf16[384,1024]{1,0:T(8,128)(2,1)} %add_convert_fusion.1) | copy-start | bytes 2359300
Sparse Core Ops, SparseCore 0:
  8.9 12.5 all-gather.6
  23.6 113.2 all-gather.8
  139.0 72.5 all-gather.10
  216.9 7.4 reduce-scatter.2
  226.8 11.0 all-gather.12
  240.0 177.2 all-gather.14
  419.5 174.2 all-gather.16
  609.3 7.0 reduce-scatter.4
